TPU v7x, 256 devices: a whole 4x4x8 slice. The times are simulated.
256 devices in a mesh: sp: 64 (over z, x, core), tp: 4 (over y).
Axes of the slice: x: 4, y: 4, z: 8, core: 2. Of those that a mesh axis runs over, the one named last changes fastest.
Arguments:
- queries: bfloat16 [32768, 2048], P('sp', 'tp'), may hold values from -90 to 90, as said below
- key_rows: bfloat16 [32768, 512], P('sp', 'tp'), may hold values from -6 to 6
- value_rows: bfloat16 [32768, 512], P('sp', 'tp'), may hold values from -6 to 6
- sink_logits: float32 [16], P('tp'), may hold values from 2 to 7
- residual: bfloat16 [32768, 2048], P('sp'), may hold values from -6 to 6
- norm_gain: float32 [2048], replicated, may hold values from 0.1 to 1.9
- out_weight: bfloat16 [2048, 2048], P('tp'), may hold values from -1.5 to 1.5
- gate_weight: bfloat16 [2048, 5632], P('sp', 'tp'), may hold values from -0.125 to 0.125
- up_weight: bfloat16 [2048, 5632], P('sp', 'tp'), may hold values from -0.125 to 0.125
- down_weight: bfloat16 [5632, 2048], P('tp', 'sp'), may hold values from -0.078125 to 0.078125
Outputs:
- mixed: bfloat16 [32768, 2048], P(('sp', 'tp'))
Inputs may be any that keep to these rules, and one draw needn't show every extreme that they name: queries are mostly of order one; some rows may be much larger.
All inputs are finite; a program needn't handle non-finite values.
Results may differ from a plain program's by a relative error of at most 0.012.
Values may be sent and summed in bfloat16 or wider, within the bound.
A program may use at most 128 MiB of HBM per device.

v0:
```python
import jax
import jax.numpy as jnp
from jax import lax
from jax.sharding import PartitionSpec as P

DH = 128
WIN = 128
EPSILON = 1e-06
MASKED = -1e30


def with_halo(cells, sides, width):
    for axis, dim in sides:
        count = lax.axis_size(axis)
        ends = count - 1
        head = lax.slice_in_dim(cells, 0, width, axis=dim)
        tail = lax.slice_in_dim(cells, cells.shape[dim] - width, cells.shape[dim], axis=dim)
        cells = jnp.concatenate(
            [
                lax.ppermute(tail, axis, [(i, (i + 1) % count) for i in range(ends)]),
                cells,
                lax.ppermute(head, axis, [((i + 1) % count, i) for i in range(ends)]),
            ],
            axis=dim,
        )
    return cells


def split_up(value, dim, size):
    before, after = (value.shape[:dim], value.shape[dim + 1 :])
    return jnp.moveaxis(value.reshape(*before, size, -1, *after), dim, 0)


def sent_and_summed(value, axis, dim):
    size = lax.axis_size(axis)
    blocks = lax.all_to_all(split_up(value, dim, size), axis, 0, 0, tiled=True)
    return jnp.sum(blocks.astype(jnp.float32), axis=0)


def sent_to_all(value, axis):
    size = lax.axis_size(axis)
    return lax.all_to_all(
        jnp.broadcast_to(value[None], (size, *value.shape)), axis, 0, 0, tiled=True
    )


def laid_out(blocks, dim):
    blocks = jnp.moveaxis(blocks, 0, dim)
    lengths = blocks.shape
    return blocks.reshape(*lengths[:dim], lengths[dim] * lengths[dim + 1], *lengths[dim + 2 :])


def gather_directly(value, axis, dim):
    blocks = sent_to_all(value, axis)
    return laid_out(blocks, dim)


def side_by_side(arrays, axis, dim, along):
    ends, at = ([], 0)
    for a in arrays[:-1]:
        at += a.shape[along]
        ends.append(at)
    both = jnp.concatenate(arrays, axis=along)
    return tuple(jnp.split(lax.all_gather(both, axis, axis=dim, tiled=True), ends, axis=along))


def attend_block(query_blk, key_blk, value_blk, sink_logits, query_pos, key_pos, seq_len):
    kv_heads = key_blk.shape[1] // DH
    group_size = query_blk.shape[1] // key_blk.shape[1]
    query_four = query_blk.reshape(query_blk.shape[0], kv_heads, group_size, DH)
    key_three = key_blk.reshape(key_blk.shape[0], kv_heads, DH)
    value_three = value_blk.reshape(value_blk.shape[0], kv_heads, DH)
    scores = jnp.einsum(
        "qhgd,khd->hgqk", query_four, key_three, preferred_element_type=jnp.float32
    ) * DH ** (-0.5)
    allowed = (
        (jnp.abs(key_pos[None, :] - query_pos[:, None]) <= WIN)
        & (key_pos[None, :] >= 0)
        & (key_pos[None, :] < seq_len)
    )
    scores = jnp.where(allowed[None, None], scores, MASKED)
    sink_col = sink_logits.reshape(kv_heads, group_size)[:, :, None]
    highest = jnp.maximum(jnp.max(scores, axis=-1), sink_col)
    weights_exp = jnp.exp(scores - highest[..., None])
    denominator = jnp.sum(weights_exp, axis=-1) + jnp.exp(sink_col - highest)
    probabilities = (weights_exp / denominator[..., None]).astype(jnp.bfloat16)
    heads_out = jnp.einsum(
        "hgqk,khd->qhgd", probabilities, value_three, preferred_element_type=jnp.float32
    )
    return heads_out.astype(jnp.bfloat16).reshape(query_blk.shape[0], kv_heads * group_size * DH)


def rms_scale(rows_wide, norm_gain):
    mean_square = jnp.mean(rows_wide * rows_wide, axis=-1, keepdims=True)
    return (rows_wide * lax.rsqrt(mean_square + EPSILON) * norm_gain).astype(jnp.bfloat16)


def fetch_down(down_weight):
    return lax.all_gather(down_weight, "sp", axis=1, tiled=True)


def shards(
    queries,
    key_rows,
    value_rows,
    sink_logits,
    residual,
    norm_gain,
    out_weight,
    gate_weight,
    up_weight,
    down_weight,
):
    tok_local = queries.shape[0]
    block_len = 2 * WIN
    share_rows = tok_local // lax.axis_size("tp")
    seq_len = tok_local * lax.axis_size("sp")
    device_offset = lax.axis_index("sp") * tok_local
    kv_pair = jnp.stack([key_rows, value_rows])
    kv_ext = with_halo(kv_pair, (("sp", 1),), WIN)

    def one_block(block_index):
        block_first = block_index * block_len
        query_blk = lax.dynamic_slice_in_dim(queries, block_first, block_len, 0)
        key_blk = lax.dynamic_slice_in_dim(kv_ext[0], block_first, block_len + 2 * WIN, 0)
        value_blk = lax.dynamic_slice_in_dim(kv_ext[1], block_first, block_len + 2 * WIN, 0)
        query_pos = device_offset + block_first + jnp.arange(block_len, dtype=jnp.int32)
        key_pos = (
            device_offset + block_first - WIN + jnp.arange(block_len + 2 * WIN, dtype=jnp.int32)
        )
        return attend_block(query_blk, key_blk, value_blk, sink_logits, query_pos, key_pos, seq_len)

    blocks = lax.map(one_block, jnp.arange(tok_local // block_len, dtype=jnp.int32))
    attended = blocks.reshape(tok_local, queries.shape[1])
    own_first = lax.axis_index("tp") * share_rows
    picked = attended
    attn_share = sent_and_summed(
        jnp.dot(picked, out_weight, preferred_element_type=jnp.float32).astype(jnp.bfloat16),
        "tp",
        0,
    )
    middle_own = (
        lax.dynamic_slice_in_dim(residual, own_first, share_rows, 0).astype(jnp.float32)
        + attn_share
    )
    normed_all = gather_directly(rms_scale(middle_own, norm_gain), "tp", 0)
    pieces = side_by_side((gate_weight, up_weight), "sp", 0, 1)
    gate_sectioned = pieces[0]
    up_sectioned = pieces[1]
    gate_acc = jnp.dot(normed_all, gate_sectioned, preferred_element_type=jnp.float32)
    up_acc = jnp.dot(normed_all, up_sectioned, preferred_element_type=jnp.float32)
    down_whole = fetch_down(down_weight)
    hidden = (jax.nn.silu(gate_acc) * up_acc).astype(jnp.bfloat16)
    picked = hidden
    ffn_share = lax.psum_scatter(
        jnp.dot(picked, down_whole, preferred_element_type=jnp.float32).astype(jnp.bfloat16),
        "tp",
        scatter_dimension=0,
        tiled=True,
    ).astype(jnp.float32)
    return (middle_own + ffn_share).astype(jnp.bfloat16)


def solution(mesh):
    placed = (
        P("sp", "tp"),
        P("sp", "tp"),
        P("sp", "tp"),
        P("tp"),
        P("sp", None),
        P(),
        P("tp", None),
        P("sp", "tp"),
        P("sp", "tp"),
        P("tp", "sp"),
    )
    return jax.shard_map(
        shards, mesh=mesh, in_specs=placed, out_specs=P(("sp", "tp"), None), check_vma=False
    )
```

profile of v0, /device:TPU:1, one launch (start us, length us, event | category | flops | bytes accessed | tf_op | source)
XLA Modules:
  0.0 233.1 jit_solution(577112236005821725)
XLA Ops:
  6.5 0.0 copy-start
  6.5 0.0 all-gather.3.cloned.1.call-start
  6.5 1.8 pad_maximum_fusion.1
  8.3 0.0 all-gather.3.cloned.1.call-update
  8.3 0.0 all-gather.5.cloned.1.call-start
  8.4 0.7 all-gather.5.cloned.1.call-update
  9.1 0.8 pad_maximum_fusion.3
  9.9 4.5 %collective-permute-start = (bf16[2,128,128]{2,1,0:T(8,128)(2,1)S(1)}, bf16[2,128,128]{2,1,0:T(8,128)(2,1)S(1)}, u32[]{:S(2)}, u32[]{:S(2)}) collective-permute-start(bf16[2,128,128]{2,1,0:T(8,128)(2,1)S(1)} %get-tuple-element.122), channel_id=1, source_target_pairs={{0,4},{4,8},{8,12},{12,16},{16,20},{20,24},{24,28},{28,32},{32,36}... | collective-permute-start | bytes 196616 | tf_op jit(solution)/shard_map/ppermute | solution.py:20
  14.4 1.9 collective-permute-start.1
  16.4 0.0 collective-permute-done
  16.4 3.6 %collective-permute-done.1 = bf16[2,128,128]{2,1,0:T(8,128)(2,1)S(1)} collective-permute-done((bf16[2,128,128]{2,1,0:T(8,128)(2,1)S(1)}, bf16[2,128,128]{2,1,0:T(8,128)(2,1)S(1)}, u32[]{:S(2)}, u32[]{:S(2)}) %collective-permute-start.1) | collective-permute-done | bytes 65568 | tf_op jit(solution)/shard_map/ppermute | solution.py:22
  20.0 1.0 pad_maximum_fusion
  21.0 11.1 %while.12 = (s32[]{:T(128)}, bf16[2,256,512]{2,1,0:T(8,128)(2,1)}, bf16[2,768,128]{2,1,0:T(8,128)(2,1)S(1)}, s32[2]{0:T(128)S(1)}, s32[]{:T(128)}, /*index=5*/bf...) while((s32[]{:T(128)}, bf16[2,256,512]{2,1,0:T(8,128)(2,1)}, ...), condition=%wide.region_3.4_spmd, body=%wide.region_0.3_spmd.sunk | while | flops 273420544 | bytes 14467520 | solution.py:133
  21.0 0.6 dynamic_slice.48
  22.3 0.3 fusion.46
  22.6 1.0 constant_dynamic-slice_fusion.2
  23.6 0.0 copy-start.2
  23.6 0.1 copy.25
  23.7 0.5 fusion.47
  24.2 0.0 copy-done.2
  24.2 0.1 broadcast_maximum_fusion.2
  24.3 0.3 fusion.48
  24.6 0.1 exponential_add_fusion.2
  24.7 0.0 copy-start.4
  24.7 0.5 convolution_convert_fusion.4
  25.2 0.1 copy.26
  25.4 0.4 copy-done.4
  25.8 0.0 copy-start.5
  25.8 0.8 copy-done.5
  26.6 0.6 dynamic_slice.48
  27.8 0.3 fusion.46
  28.1 1.0 constant_dynamic-slice_fusion.2
  29.1 0.0 copy-start.2
  29.1 0.1 copy.25
  29.3 0.5 fusion.47
  29.8 0.0 copy-done.2
  29.8 0.1 broadcast_maximum_fusion.2
  29.8 0.3 fusion.48
  30.1 0.1 exponential_add_fusion.2
  30.2 0.5 convolution_convert_fusion.4
  30.8 0.1 copy.26
  30.9 0.4 copy-done.4
  31.3 0.0 copy-start.5
  31.3 0.8 copy-done.5
  32.1 0.0 copy-done
  32.1 3.6 %convolution_convert_fusion.1 = bf16[512,2048]{1,0:T(8,128)(2,1)} fusion(bf16[512,512]{1,0:T(8,128)(2,1)} %bitcast.59, bf16[512,2048]{1,0:T(8,128)(2,1)S(1)} %copy-done), kind=kOutput, calls=%fused_computation.30 | convolution fusion | flops 1074790400 | bytes 4718592 | tf_op jit(solution)/shard_map/dot_general | solution.py:138
  35.7 4.4 %all-to-all-start = ((bf16[4,128,2048]{2,1,0:T(8,128)(2,1)}), bf16[4,128,2048]{2,1,0:T(8,128)(2,1)}, u32[]{:S(2)}, u32[]{:S(2)}) async-start(bf16[4,128,2048]{2,1,0:T(8,128)(2,1)} %bitcast.52), calls=%async_computation | async-start | bytes 4194304 | tf_op jit(solution)/shard_map/all_to_all | solution.py:36
  40.2 0.0 reduce-scatter.2.cloned.1.call-start
  40.2 0.0 copy-start.3
  40.2 24.7 %all-to-all-done = bf16[4,128,2048]{2,1,0:T(8,128)(2,1)} async-done(((bf16[4,128,2048]{2,1,0:T(8,128)(2,1)}), bf16[4,128,2048]{2,1,0:T(8,128)(2,1)}, u32[]{:S(2)}, u32[]{:S(2)}) %all-to-all-start) | async-done | bytes 2097184 | tf_op jit(solution)/shard_map/all_to_all | solution.py:36
  64.9 2.2 convert_reduce_fusion
  67.1 0.0 copy-done.1
  67.2 0.2 multiply_reduce_fusion
  67.4 0.0 copy-done.3
  67.4 0.2 multiply_convert_fusion
  67.6 0.2 broadcast_in_dim.44
  67.9 30.0 %all_to_all.10 = bf16[4,128,2048]{2,1,0:T(8,128)(2,1)} all-to-all(bf16[4,128,2048]{2,1,0:T(8,128)(2,1)S(1)} %broadcast_in_dim.44), channel_id=1, replica_groups=mesh['sp'=64,'tp'=4] {'tp'}, dimensions={0} | all-to-all | bytes 4194304 | tf_op jit(solution)/shard_map/all_to_all | solution.py:42
  97.9 4.1 %all-gather.3.cloned.1.call-done = bf16[2048,2816]{1,0:T(8,128)(2,1)} async-done(((bf16[32,2816]{1,0:T(8,128)(2,1)}), bf16[2048,2816]{1,0:T(8,128)(2,1)}) %all-gather.3.cloned.1.call-update) | async-done | bytes 11534352 | tf_op jit(solution)/shard_map/all_gather | solution.py:64
  102.0 8.2 %fusion.14 = f32[512,1408]{1,0:T(8,128)} fusion(bf16[512,2048]{1,0:T(8,128)(2,1)} %bitcast.53, bf16[2048,2816]{1,0:T(8,128)(2,1)} %all-gather.3.cloned.1.call-done), kind=kOutput, calls=%fused_computation.25 | convolution fusion | flops 2952790016 | bytes 10747904 | tf_op jit(solution)/shard_map/dot_general | solution.py:150
  110.2 71.3 %all-gather.5.cloned.1.call-done = bf16[1408,2048]{0,1:T(8,128)(2,1)} async-done(((bf16[1408,32]{0,1:T(8,128)(2,1)}), bf16[1408,2048]{0,1:T(8,128)(2,1)}) %all-gather.5.cloned.1.call-update) | async-done | bytes 5767184 | tf_op jit(solution)/shard_map/all_gather | solution.py:99
  181.5 13.8 %convolution_convert_fusion.2 = bf16[512,2048]{1,0:T(8,128)(2,1)} fusion(bf16[1408,2048]{0,1:T(8,128)(2,1)} %all-gather.5.cloned.1.call-done, bf16[512,2048]{1,0:T(8,128)(2,1)} %bitcast.54, bf16[2048,2816]{1,0:T(8,128)(2,1)} %all-gather.3.cloned.1.call-done, f32[512,1408]{1,0:T(8,128)} %fusion.14), kind=kOutput, calls=%fused_computation.31 | convolution fusion | flops 5910953984 | bytes 18612224 | tf_op jit(solution)/shard_map/dot_general | solution.py:156
  195.4 0.0 reduce-scatter.2.cloned.1.call-update
  195.4 29.0 %reduce-scatter.2.cloned.1.call-done = bf16[128,2048]{1,0:T(8,128)(2,1)} async-done(((bf16[512,2048]{1,0:T(8,128)(2,1)}), bf16[128,2048]{1,0:T(8,128)(2,1)}) %reduce-scatter.2.cloned.1.call-update) | async-done | bytes 524304 | tf_op jit(solution)/shard_map/reduce_scatter | solution.py:155
  224.4 2.2 add_convert_fusion
  (15 shorter events, 0.2 us)
Async XLA Ops:
  6.5 25.6 %copy-start = (bf16[512,2048]{1,0:T(8,128)(2,1)S(1)}, bf16[512,2048]{1,0:T(8,128)(2,1)}, u32[]{:S(2)}) copy-start(bf16[512,2048]{1,0:T(8,128)(2,1)} %param.18) | copy-start | bytes 6291460
  6.5 95.5 %all-gather.3.cloned.1.call-start = ((), (), s32[]{:S(2)}) async-start(), calls=%async_computation.3 | async-start | bytes 11714560 | tf_op jit(solution)/shard_map/all_gather | solution.py:64
  8.3 173.2 %all-gather.5.cloned.1.call-start = ((), (), s32[]{:S(2)}) async-start(), calls=%async_computation.4 | async-start | bytes 5857280 | tf_op jit(solution)/shard_map/all_gather | solution.py:99
  9.9 6.5 %collective-permute-start = (bf16[2,128,128]{2,1,0:T(8,128)(2,1)S(1)}, bf16[2,128,128]{2,1,0:T(8,128)(2,1)S(1)}, u32[]{:S(2)}, u32[]{:S(2)}) collective-permute-start(bf16[2,128,128]{2,1,0:T(8,128)(2,1)S(1)} %get-tuple-element.122), channel_id=1, source_target_pairs={{0,4},{4,8},{8,12},{12,16},{16,20},{20,24},{24,28},{28,32},{32,36}... | collective-permute-start | bytes 196616 | tf_op jit(solution)/shard_map/ppermute | solution.py:20
  14.4 5.6 %collective-permute-start.1 = (bf16[2,128,128]{2,1,0:T(8,128)(2,1)S(1)}, bf16[2,128,128]{2,1,0:T(8,128)(2,1)S(1)}, u32[]{:S(2)}, u32[]{:S(2)}) collective-permute-start(bf16[2,128,128]{2,1,0:T(8,128)(2,1)S(1)} %get-tuple-element.123), channel_id=1, source_target_pairs={{4,0},{8,4},{12,8},{16,12},{20,16},{24,20},{28,24},{32,28},{36,32}... | collective-permute-start | bytes 196616 | tf_op jit(solution)/shard_map/ppermute | solution.py:22
  23.6 0.7 copy-start.2
  24.7 1.0 copy-start.4
  25.8 0.8 copy-start.5
  29.1 0.7 copy-start.2
  30.2 1.0 copy-start.4
  31.3 0.8 copy-start.5
  35.7 29.2 %all-to-all-start = ((bf16[4,128,2048]{2,1,0:T(8,128)(2,1)}), bf16[4,128,2048]{2,1,0:T(8,128)(2,1)}, u32[]{:S(2)}, u32[]{:S(2)}) async-start(bf16[4,128,2048]{2,1,0:T(8,128)(2,1)} %bitcast.52), calls=%async_computation | async-start | bytes 4194304 | tf_op jit(solution)/shard_map/all_to_all | solution.py:36
  40.2 184.2 %reduce-scatter.2.cloned.1.call-start = ((), (), s32[]{:S(2)}) async-start(), calls=%async_computation.5 | async-start | bytes 2621440 | tf_op jit(solution)/shard_map/reduce_scatter | solution.py:155
  40.2 27.2 %copy-start.3 = (f32[2048]{0:T(1024)S(1)}, f32[2048]{0:T(1024)}, u32[]{:S(2)}) copy-start(f32[2048]{0:T(1024)} %param.17) | copy-start | bytes 24580
  64.9 2.2 copy-start.1
Sparse Core Ops, SparseCore 0:
  10.1 91.8 all-gather.2
  104.7 76.7 all-gather.4
  195.5 28.8 reduce-scatter.1
where the time goes:
time: 234 us; the launch traced here: 233 us
  waiting for transfers between devices  133 us (57%)
  blocking collectives  30 us (13%)
  matrix products  27.7 us (12%)
  between operations  13.2 us (6%)
  starting transfers between devices  10.9 us (5%)
  other arithmetic  9.91 us (4%)
  local copies, waits for them, and re-layouts  6.4 us (3%)
    all_gather x1, waiting for transfers between devices, fetch_down(): return lax.all_gather(down_weight, 'sp', axis=1, tiled=True)  71.3 us
    all_to_all x1, blocking collectives, sent_to_all(): lax.all_to_all(jnp.broadcast_to(value[None], (size, *value.shape)), axis,...  30 us
    reduce_scatter x1, waiting for transfers between devices, shards(): lax.psum_scatter(jnp.dot(picked, down_whole, preferred_element_type=jnp.f...  29 us
    all_to_all x1, waiting for transfers between devices, sent_and_summed(): blocks = lax.all_to_all(split_up(value, dim, size), axis, 0, 0, tiled=True)  24.7 us
    dot_general x1, matrix products, shards(): jnp.dot(picked, down_whole, preferred_element_type=jnp.float32)  13.8 us
    dot_general x1, matrix products, shards(): jnp.dot(normed_all, gate_sectioned, preferred_element_type=jnp.float32)  8.23 us
  transfers between devices with their start and end apart: 6, of which 5 were waited for; matrix products, arithmetic and copies ran while one was open for 10% of the time, Pallas kernels for 0%

commit v1 on v0

--- a/solution.py
+++ b/solution.py
@@ -96,7 +96,9 @@
 
 
 def fetch_down(down_weight):
-    return lax.all_gather(down_weight, "sp", axis=1, tiled=True)
+    return jnp.concatenate(
+        lax.all_to_all(jnp.stack([down_weight] * lax.axis_size("sp")), "sp", 0, 0), axis=1
+    )
 
 
 def shards(

time: 234 us -> 293 us (1.25)
  waiting for transfers between devices: 133 us -> 176 us
  starting transfers between devices: 10.9 us -> 26.7 us
    all_to_all x0 -> x1, waiting for transfers between devices: none -> 119 us  [fetch_down(): lax.all_to_all(jnp.stack([down_weight] * lax.axis_size('sp')), 'sp', 0, 0)]
    all_gather x1 -> x0, waiting for transfers between devices: 71.3 us -> none  [fetch_down(): return lax.all_gather(down_weight, 'sp', axis=1, tiled=True)]
    all_to_all x0 -> x1, starting transfers between devices: none -> 15 us  [fetch_down(): lax.all_to_all(jnp.stack([down_weight] * lax.axis_size('sp')), 'sp', 0, 0)]
    all_gather x1, waiting for transfers between devices: 4.12 us -> 0.02 us  [side_by_side(): lax.all_gather(both, axis, axis=dim, tiled=True)]
    ppermute x1, waiting for transfers between devices: 3.63 us -> 0.01 us  [with_halo(): lax.ppermute(head, axis, [((i + 1) % count, i) for i in range(ends)])]
    ppermute x1, starting transfers between devices: 1.92 us -> 5.11 us  [with_halo(): lax.ppermute(head, axis, [((i + 1) % count, i) for i in range(ends)])]
  transfers between devices with their start and end apart: 6 -> 6, of which waited for: 5 -> 4; matrix products, arithmetic and copies ran while one was open for 10% -> 10% of each run, Pallas kernels for 0% -> 0%
where the time goes in v1:
time: 293 us
  waiting for transfers between devices  176 us (60%)
  blocking collectives  28.7 us (10%)
  matrix products  27.8 us (9%)
  starting transfers between devices  26.7 us (9%)
  between operations  13.5 us (5%)
  other arithmetic  10.2 us (3%)
  local copies, waits for them, and re-layouts  8.63 us (3%)
    all_to_all x1, waiting for transfers between devices, fetch_down(): lax.all_to_all(jnp.stack([down_weight] * lax.axis_size('sp')), 'sp', 0, 0)  119 us
    all_to_all x1, blocking collectives, sent_to_all(): lax.all_to_all(jnp.broadcast_to(value[None], (size, *value.shape)), axis,...  28.7 us
    reduce_scatter x1, waiting for transfers between devices, shards(): lax.psum_scatter(jnp.dot(picked, down_whole, preferred_element_type=jnp.f...  28.7 us
    all_to_all x1, waiting for transfers between devices, sent_and_summed(): blocks = lax.all_to_all(split_up(value, dim, size), axis, 0, 0, tiled=True)  26.4 us
    all_to_all x1, starting transfers between devices, fetch_down(): lax.all_to_all(jnp.stack([down_weight] * lax.axis_size('sp')), 'sp', 0, 0)  15 us
    dot_general x1, matrix products, shards(): jnp.dot(picked, down_whole, preferred_element_type=jnp.float32)  13.8 us
    dot_general x1, matrix products, shards(): jnp.dot(normed_all, gate_sectioned, preferred_element_type=jnp.float32)  8.3 us
  transfers between devices with their start and end apart: 6, of which 4 were waited for; matrix products, arithmetic and copies ran while one was open for 10% of the time, Pallas kernels for 0%

profile of v1, /device:TPU:1, one launch (start us, length us, event | category | flops | bytes accessed | tf_op | source)
XLA Modules:
  0.0 292.9 jit_solution(17788284408751387814)
XLA Ops:
  6.5 0.0 copy-start
  6.5 0.0 all-gather.2.cloned.1.call-start
  6.5 1.8 pad_maximum_fusion.1
  8.3 0.0 all-gather.2.cloned.1.call-update
  8.3 0.8 pad_maximum_fusion.3
  9.2 5.1 %collective-permute-start.1 = (bf16[2,128,128]{2,1,0:T(8,128)(2,1)S(1)}, bf16[2,128,128]{2,1,0:T(8,128)(2,1)S(1)}, u32[]{:S(2)}, u32[]{:S(2)}) collective-permute-start(bf16[2,128,128]{2,1,0:T(8,128)(2,1)S(1)} %get-tuple-element.123), channel_id=1, source_target_pairs={{4,0},{8,4},{12,8},{16,12},{20,16},{24,20},{28,24},{32,28},{36,32}... | collective-permute-start | bytes 196616 | tf_op jit(solution)/shard_map/ppermute | solution.py:22
  14.3 1.9 collective-permute-start
  16.2 0.0 collective-permute-done.1
  16.2 1.3 collective-permute-done
  17.5 1.0 pad_maximum_fusion
  18.5 10.5 %while.12 = (s32[]{:T(128)}, bf16[2,256,512]{2,1,0:T(8,128)(2,1)}, bf16[2,768,128]{2,1,0:T(8,128)(2,1)S(1)}, s32[2]{0:T(128)S(1)}, s32[]{:T(128)}, /*index=5*/bf...) while((s32[]{:T(128)}, bf16[2,256,512]{2,1,0:T(8,128)(2,1)}, ...), condition=%wide.region_3.4_spmd, body=%wide.region_0.3_spmd.sunk | while | flops 273420544 | bytes 10273160 | solution.py:135
  18.5 0.7 dynamic_slice.48
  19.9 1.0 constant_dynamic-slice_fusion.2
  20.9 0.0 copy-start.3
  20.9 0.1 copy.26
  21.1 0.3 fusion.46
  21.4 0.5 fusion.47
  21.9 0.0 copy-done.3
  21.9 0.1 broadcast_maximum_fusion.2
  22.0 0.3 fusion.48
  22.3 0.1 exponential_add_fusion.2
  22.3 0.5 convolution_convert_fusion.4
  22.9 0.1 copy.27
  23.0 0.7 constant_dynamic-update-slice_fusion.2
  23.8 0.7 dynamic_slice.48
  25.1 1.0 constant_dynamic-slice_fusion.2
  26.1 0.0 copy-start.3
  26.1 0.1 copy.26
  26.4 0.3 fusion.46
  26.6 0.5 fusion.47
  27.1 0.0 copy-done.3
  27.1 0.1 broadcast_maximum_fusion.2
  27.2 0.3 fusion.48
  27.5 0.1 exponential_add_fusion.2
  27.6 0.5 convolution_convert_fusion.4
  28.1 0.1 copy.27
  28.3 0.7 constant_dynamic-update-slice_fusion.2
  29.0 0.0 copy-done
  29.0 3.6 %convolution_convert_fusion.1 = bf16[512,2048]{1,0:T(8,128)(2,1)} fusion(bf16[512,512]{1,0:T(8,128)(2,1)} %bitcast.62, bf16[512,2048]{1,0:T(8,128)(2,1)S(1)} %copy-done), kind=kOutput, calls=%fused_computation.30 | convolution fusion | flops 1074790400 | bytes 4718592 | tf_op jit(solution)/shard_map/dot_general | solution.py:140
  32.6 4.4 %all-to-all-start = ((bf16[4,128,2048]{2,1,0:T(8,128)(2,1)}), bf16[4,128,2048]{2,1,0:T(8,128)(2,1)}, u32[]{:S(2)}, u32[]{:S(2)}) async-start(bf16[4,128,2048]{2,1,0:T(8,128)(2,1)} %bitcast.55), calls=%async_computation | async-start | bytes 4194304 | tf_op jit(solution)/shard_map/all_to_all | solution.py:36
  37.0 0.0 copy-start.4
  37.1 26.4 %all-to-all-done = bf16[4,128,2048]{2,1,0:T(8,128)(2,1)} async-done(((bf16[4,128,2048]{2,1,0:T(8,128)(2,1)}), bf16[4,128,2048]{2,1,0:T(8,128)(2,1)}, u32[]{:S(2)}, u32[]{:S(2)}) %all-to-all-start) | async-done | bytes 2097184 | tf_op jit(solution)/shard_map/all_to_all | solution.py:36
  63.5 0.0 copy-start.1
  63.5 2.5 convert_reduce_fusion
  66.0 0.1 copy-done.1
  66.1 0.2 multiply_reduce_fusion
  66.3 0.0 copy-done.4
  66.3 0.2 multiply_convert_fusion
  66.6 0.2 broadcast_in_dim.44
  66.8 0.0 copy-start.2
  66.8 28.7 %all_to_all.15 = bf16[4,128,2048]{2,1,0:T(8,128)(2,1)} all-to-all(bf16[4,128,2048]{2,1,0:T(8,128)(2,1)S(1)} %broadcast_in_dim.44), channel_id=1, replica_groups=mesh['sp'=64,'tp'=4] {'tp'}, dimensions={0} | all-to-all | bytes 4194304 | tf_op jit(solution)/shard_map/all_to_all | solution.py:42
  95.6 0.0 copy-done.2
  95.6 2.9 stack.11
  98.5 15.0 %all-to-all-start.2 = ((bf16[64,1408,32]{1,2,0:T(8,128)(2,1)}), bf16[64,1408,32]{1,2,0:T(8,128)(2,1)}, u32[]{:S(2)}, u32[]{:S(2)}) async-start(bf16[64,1408,32]{1,2,0:T(8,128)(2,1)} %stack.11), calls=%async_computation.2 | async-start | bytes 11534336 | tf_op jit(solution)/shard_map/all_to_all | solution.py:100
  113.5 0.2 reduce-scatter.2.cloned.1.call-start
  113.7 0.0 all-gather.2.cloned.1.call-done
  113.7 8.3 %fusion.14 = f32[512,1408]{1,0:T(8,128)} fusion(bf16[512,2048]{1,0:T(8,128)(2,1)} %bitcast.56, bf16[2048,2816]{1,0:T(8,128)(2,1)} %all-gather.2.cloned.1.call-done), kind=kOutput, calls=%fused_computation.25 | convolution fusion | flops 2952790016 | bytes 10747904 | tf_op jit(solution)/shard_map/dot_general | solution.py:152
  122.0 119.2 %all-to-all-done.2 = bf16[64,1408,32]{1,2,0:T(8,128)(2,1)} async-done(((bf16[64,1408,32]{1,2,0:T(8,128)(2,1)}), bf16[64,1408,32]{1,2,0:T(8,128)(2,1)}, u32[]{:S(2)}, u32[]{:S(2)}) %all-to-all-start.2) | async-done | bytes 5767200 | tf_op jit(solution)/shard_map/all_to_all | solution.py:100
  241.2 13.8 %convolution_convert_fusion.2 = bf16[512,2048]{1,0:T(8,128)(2,1)} fusion(bf16[1408,2048]{0,1:T(8,128)(2,1)} %bitcast.18, bf16[512,2048]{1,0:T(8,128)(2,1)} %bitcast.57, bf16[2048,2816]{1,0:T(8,128)(2,1)} %all-gather.2.cloned.1.call-done, f32[512,1408]{1,0:T(8,128)} %fusion.14), kind=kOutput, calls=%fused_computation.31 | convolution fusion | flops 5910953984 | bytes 18612224 | tf_op jit(solution)/shard_map/dot_general | solution.py:158
  255.1 0.0 reduce-scatter.2.cloned.1.call-update
  255.1 28.7 %reduce-scatter.2.cloned.1.call-done = bf16[128,2048]{1,0:T(8,128)(2,1)} async-done(((bf16[512,2048]{1,0:T(8,128)(2,1)}), bf16[128,2048]{1,0:T(8,128)(2,1)}) %reduce-scatter.2.cloned.1.call-update) | async-done | bytes 524304 | tf_op jit(solution)/shard_map/reduce_scatter | solution.py:157
  283.8 2.2 add_convert_fusion
  (11 shorter events, 0.1 us)
Async XLA Ops:
  6.5 22.5 %copy-start = (bf16[512,2048]{1,0:T(8,128)(2,1)S(1)}, bf16[512,2048]{1,0:T(8,128)(2,1)}, u32[]{:S(2)}) copy-start(bf16[512,2048]{1,0:T(8,128)(2,1)} %param.18) | copy-start | bytes 6291460
  6.5 107.2 %all-gather.2.cloned.1.call-start = ((), (), s32[]{:S(2)}) async-start(), calls=%async_computation.4 | async-start | bytes 11714560 | tf_op jit(solution)/shard_map/all_gather | solution.py:64
  9.2 7.1 %collective-permute-start.1 = (bf16[2,128,128]{2,1,0:T(8,128)(2,1)S(1)}, bf16[2,128,128]{2,1,0:T(8,128)(2,1)S(1)}, u32[]{:S(2)}, u32[]{:S(2)}) collective-permute-start(bf16[2,128,128]{2,1,0:T(8,128)(2,1)S(1)} %get-tuple-element.123), channel_id=1, source_target_pairs={{4,0},{8,4},{12,8},{16,12},{20,16},{24,20},{28,24},{32,28},{36,32}... | collective-permute-start | bytes 196616 | tf_op jit(solution)/shard_map/ppermute | solution.py:22
  14.3 3.2 %collective-permute-start = (bf16[2,128,128]{2,1,0:T(8,128)(2,1)S(1)}, bf16[2,128,128]{2,1,0:T(8,128)(2,1)S(1)}, u32[]{:S(2)}, u32[]{:S(2)}) collective-permute-start(bf16[2,128,128]{2,1,0:T(8,128)(2,1)S(1)} %get-tuple-element.122), channel_id=1, source_target_pairs={{0,4},{4,8},{8,12},{12,16},{16,20},{20,24},{24,28},{28,32},{32,36}... | collective-permute-start | bytes 196616 | tf_op jit(solution)/shard_map/ppermute | solution.py:20
  20.9 1.0 copy-start.3
  26.1 1.0 copy-start.3
  32.6 30.9 %all-to-all-start = ((bf16[4,128,2048]{2,1,0:T(8,128)(2,1)}), bf16[4,128,2048]{2,1,0:T(8,128)(2,1)}, u32[]{:S(2)}, u32[]{:S(2)}) async-start(bf16[4,128,2048]{2,1,0:T(8,128)(2,1)} %bitcast.55), calls=%async_computation | async-start | bytes 4194304 | tf_op jit(solution)/shard_map/all_to_all | solution.py:36
  37.0 29.3 %copy-start.4 = (f32[2048]{0:T(1024)S(1)}, f32[2048]{0:T(1024)}, u32[]{:S(2)}) copy-start(f32[2048]{0:T(1024)} %param.17) | copy-start | bytes 24580
  63.5 2.6 copy-start.1
  66.8 28.7 %copy-start.2 = (bf16[1408,32]{0,1:T(8,128)(2,1)S(1)}, bf16[1408,32]{0,1:T(8,128)(2,1)}, u32[]{:S(2)}) copy-start(bf16[1408,32]{0,1:T(8,128)(2,1)} %param.21) | copy-start | bytes 270340
  98.5 142.8 %all-to-all-start.2 = ((bf16[64,1408,32]{1,2,0:T(8,128)(2,1)}), bf16[64,1408,32]{1,2,0:T(8,128)(2,1)}, u32[]{:S(2)}, u32[]{:S(2)}) async-start(bf16[64,1408,32]{1,2,0:T(8,128)(2,1)} %stack.11), calls=%async_computation.2 | async-start | bytes 11534336 | tf_op jit(solution)/shard_map/all_to_all | solution.py:100
  113.5 170.4 %reduce-scatter.2.cloned.1.call-start = ((), (), s32[]{:S(2)}) async-start(), calls=%async_computation.5 | async-start | bytes 2621440 | tf_op jit(solution)/shard_map/reduce_scatter | solution.py:157
Sparse Core Ops, SparseCore 0:
  10.1 91.8 all-gather.1
  255.2 28.5 reduce-scatter.1
